TPU v7x, 512 devices: a whole 4x8x8 slice. The times are simulated.
512 devices in a mesh: rep: 2 (over z_hi), fs: 32 (over z_lo, y), tp: 8 (over x, core).
Axes of the slice: x: 4, y: 8, z: 8 (z_hi: 2, z_lo: 4; z = z_hi * 4 + z_lo), core: 2. Of those that a mesh axis runs over, the one named last changes fastest.
Arguments:
- states: bfloat16 [24576, 2048], P(('rep', 'fs'), 'tp'), may hold values from -6 to 6
- mix_gain: float32 [2048], replicated, may hold values from 0.1 to 1.9
- w_value: bfloat16 [2048, 2048], P('fs', 'tp'), may hold values from -1 to 1
- w_gate: bfloat16 [2048, 2048], P('fs', 'tp'), may hold values from -0.125 to 0.125
- conv_kernel: float32 [31, 2048], replicated, may hold values from -1 to 1
- chan_gain: float32 [2048], replicated, may hold values from 0.1 to 1.9
- w_mix_out: bfloat16 [2048, 2048], P('fs', 'tp'), may hold values from -0.125 to 0.125
- mlp_gain: float32 [2048], replicated, may hold values from 0.1 to 1.9
- w_up: bfloat16 [2048, 6144], P('fs', 'tp'), may hold values from -0.125 to 0.125
- w_down_t: bfloat16 [2048, 6144], P('fs', 'tp'), may hold values from -0.078125 to 0.078125
Outputs:
- layer_out: bfloat16 [24576, 2048], P(('rep', 'fs'), 'tp')
All inputs are finite; a program needn't handle non-finite values.
Results may differ from a plain program's by a relative error of at most 0.017.
Values may be sent and summed in bfloat16 or wider, within the bound.
No kernel may reach another device: no remote copies, remote signals or barrier semaphores. Data moves between devices by JAX's collectives and lax.ppermute only.
A program may use at most 64 MiB of HBM per device.

v0:
```python
import jax
import jax.numpy as jnp
from jax import lax
from jax.sharding import Mesh
from jax.sharding import PartitionSpec as P

D = 2048
KWIDTH = 31
LENGTH = 128
TP = ("tp_0", "tp_1")
EPS = 1e-06


def cut_rows(length, count):
    hop = length // count
    if hop >= 8:
        hop -= hop % 8
    return [hop * k for k in range(1, count)]


def gather_in_order(shard, axes, order):
    pieces = shard
    for k in order:
        pieces = lax.all_gather(pieces, axes[k])
    done = order[::-1]
    back = [done.index(k) for k in range(len(axes))]
    pieces = pieces.transpose(*back, *range(len(axes), pieces.ndim))
    return pieces.reshape(-1, *shard.shape)


def laid_out(pieces, dim):
    pieces = jnp.moveaxis(pieces, 0, dim)
    dims = pieces.shape
    return pieces.reshape(*dims[:dim], dims[dim] * dims[dim + 1], *dims[dim + 2 :])


def gather_at_once(shard, axes, dim):
    split_at = max(range(max(1, shard.ndim - 1)), key=lambda d: shard.shape[d])
    count, outs = (len(axes), [])
    for initial, slab in enumerate(
        jnp.split(shard, cut_rows(shard.shape[split_at], count), axis=split_at)
    ):
        if slab.size:
            order = [(initial - k) % count for k in range(count)]
            outs.append(gather_in_order(slab, axes, order))
    return laid_out(jnp.concatenate(outs, axis=split_at + 1), dim)


def half_of(weight):
    width = weight.shape[1] // 2
    return lax.dynamic_slice_in_dim(weight, lax.axis_index("rep") * width, width, 1)


def whole_halves(weights):
    mine = jnp.concatenate([half_of(w) for w in weights], axis=1)
    pieces = lax.all_gather(mine, ("rep", "fs"), axis=0, tiled=True)
    pieces = pieces.reshape(2, -1, mine.shape[1])
    ends, at = ([], 0)
    for w in weights[:-1]:
        at += w.shape[1] // 2
        ends.append(at)
    return [jnp.split(pieces[r], ends, axis=1) for r in range(2)]


def copy_for_each(shard, axis):
    copies = jnp.broadcast_to(shard, (lax.axis_size(axis), *shard.shape))
    return lax.all_to_all(copies, axis, split_axis=0, concat_axis=0, tiled=True)


def over_copies(shard, axis):
    everything = copy_for_each(shard, axis)
    return jnp.sum(everything, axis=0)


def in_one(arrays, axis):
    ends = [0]
    for a in arrays:
        ends.append(ends[-1] + a.size)
    so_far = over_copies(jnp.concatenate([a.ravel() for a in arrays]), axis)
    return tuple((so_far[b:e].reshape(a.shape) for a, b, e in zip(arrays, ends, ends[1:])))


def in_blocks(shard, dim, count):
    before, after = (shard.shape[:dim], shard.shape[dim + 1 :])
    return jnp.moveaxis(shard.reshape(*before, count, -1, *after), dim, 0)


def summed_on_arrival(shard, axis, dim):
    count = lax.axis_size(axis)
    pieces = lax.all_to_all(in_blocks(shard, dim, count), axis, 0, 0, tiled=True)
    return jnp.sum(pieces.astype(jnp.float32), axis=0)


def collect(shard, axis, dim):
    pieces = copy_for_each(shard, axis)
    return laid_out(pieces, dim)


def rms_norm(rows, gain):
    values = rows.astype(jnp.float32)
    scaled = values * lax.rsqrt(jnp.mean(values * values, axis=-1, keepdims=True) + EPS)
    return (scaled * gain).astype(jnp.bfloat16)


def times_transposed(left, right):
    return lax.dot_general(
        left, right, (((1,), (1,)), ((), ())), preferred_element_type=jnp.float32
    )


def body(
    states, mix_gain, w_value, w_gate, conv_kernel, chan_gain, w_mix_out, mlp_gain, w_up, w_down_t
):
    width = states.shape[1]
    offset = lax.axis_index(TP) * width
    token_rows = states.shape[0]
    whole_rows = gather_at_once(states, TP, 1)
    normed = rms_norm(whole_rows, mix_gain)
    mix = whole_halves((w_value, w_gate, w_mix_out))
    value = jnp.concatenate(
        [jnp.dot(normed, h[0], preferred_element_type=jnp.float32) for h in mix], axis=1
    )
    gate = jnp.concatenate(
        [jnp.dot(normed, h[1], preferred_element_type=jnp.float32) for h in mix], axis=1
    )
    gated = value * jax.nn.sigmoid(gate)
    own_kernel = lax.dynamic_slice_in_dim(conv_kernel, offset, width, 1)
    blocks = gated.reshape(token_rows // LENGTH, LENGTH, width)
    padded = jnp.pad(blocks, ((0, 0), (KWIDTH - 1, 0), (0, 0)))
    filtered = jnp.zeros_like(blocks)
    for tap in range(KWIDTH):
        filtered = filtered + own_kernel[tap][None, None, :] * padded[:, tap : tap + LENGTH, :]
    filtered = filtered.reshape(token_rows, width)
    sum_rows, square_rows = in_one(
        (jnp.sum(filtered, axis=-1), jnp.sum(filtered * filtered, axis=-1)), TP
    )
    mean_rows = (sum_rows / D)[:, None]
    variance = (square_rows / D)[:, None] - mean_rows * mean_rows
    own_gain = lax.dynamic_slice_in_dim(chan_gain, offset, width, 0)
    activated = jax.nn.silu((filtered - mean_rows) * lax.rsqrt(variance + EPS) * own_gain).astype(
        jnp.bfloat16
    )
    mixer_terms = times_transposed(activated, jnp.concatenate([h[2] for h in mix], axis=1))
    mixed = summed_on_arrival(mixer_terms.astype(jnp.bfloat16), TP, 1)
    middle = (states.astype(jnp.float32) + mixed).astype(jnp.bfloat16)
    middle_rows = collect(middle, TP, 1)
    normed_mid = rms_norm(middle_rows, mlp_gain)
    fed_terms = 0.0
    for up, down in whole_halves((w_up, w_down_t)):
        upward = jnp.dot(normed_mid, up, preferred_element_type=jnp.float32)
        hidden = jnp.square(jnp.maximum(upward, 0.0)).astype(jnp.bfloat16)
        fed_terms = fed_terms + times_transposed(hidden, down)
    fed = summed_on_arrival(fed_terms.astype(jnp.bfloat16), TP, 1)
    return (middle.astype(jnp.float32) + fed).astype(jnp.bfloat16)


def solution(mesh):
    split = Mesh(
        mesh.devices.reshape(mesh.shape["rep"], mesh.shape["fs"], 4, 2),
        ("rep", "fs", "tp_0", "tp_1"),
    )
    return jax.shard_map(
        body,
        mesh=split,
        in_specs=(
            P(("rep", "fs"), TP),
            P(),
            P("fs", TP),
            P("fs", TP),
            P(),
            P(),
            P("fs", TP),
            P(),
            P("fs", TP),
            P("fs", TP),
        ),
        out_specs=P(("rep", "fs"), TP),
        check_vma=False,
    )
```

profile of v0, /device:TPU:1, one launch (start us, length us, event | category | flops | bytes accessed | tf_op | source)
XLA Modules:
  0.0 234.6 jit_solution(18182806777791911851)
XLA Ops:
  6.5 0.0 copy-start
  6.5 0.0 all-gather.7.cloned.1.call-start
  6.5 0.8 copy-done
  7.3 0.7 constant_dynamic-slice_fusion.3
  8.0 0.6 pad_maximum_fusion.2
  8.7 0.0 all-gather.7.cloned.1.call-update
  8.7 0.0 all-gather.9.cloned.1.call-start
  8.7 0.8 constant_dynamic-slice_fusion.1
  9.6 0.7 pad_maximum_fusion.1
  10.2 0.0 all-gather.9.cloned.1.call-update
  10.3 1.0 fusion.113
  11.2 10.8 %all-gather = bf16[768,256]{1,0:T(8,128)(2,1)S(1)} all-gather(bf16[192,256]{1,0:T(8,128)(2,1)S(1)} %get-tuple-element.41), channel_id=2, replica_groups=mesh['rep'=2,'fs'=32,'tp_0'=4,'tp_1'=2] {'tp_0'}, dimensions={0}, use_global_device_ids=true | all-gather | bytes 491520 | tf_op jit(solution)/shard_map/all_gather | solution.py:24
  22.0 10.5 %all-gather.1 = bf16[8,192,256]{2,1,0:T(8,128)(2,1)S(1)} all-gather(bf16[4,192,256]{2,1,0:T(8,128)(2,1)S(1)} %bitcast.103), channel_id=3, replica_groups=mesh['rep'=2,'fs'=32,'tp_0'=4,'tp_1'=2] {'tp_1'}, dimensions={0}, use_global_device_ids=true | all-gather | bytes 1179648 | tf_op jit(solution)/shard_map/all_gather | solution.py:24
  32.6 0.1 copy.52
  32.6 0.0 copy-start.1
  32.6 2.0 all-gather.2
  34.6 11.2 %all-gather.3 = bf16[8,192,256]{2,1,0:T(8,128)(2,1)S(1)} all-gather(bf16[2,192,256]{2,1,0:T(8,128)(2,1)S(1)} %bitcast.104), channel_id=5, replica_groups=mesh['rep'=2,'fs'=32,'tp_0'=4,'tp_1'=2] {'tp_0'}, dimensions={0}, use_global_device_ids=true | all-gather | bytes 983040 | tf_op jit(solution)/shard_map/all_gather | solution.py:24
  45.8 0.0 copy-start.2
  45.8 0.0 copy-done.1
  45.8 0.9 copy-done.2
  46.7 0.3 convert_bitcast_fusion
  47.0 1.8 copy.53
  48.9 0.0 copy-start.4
  48.9 2.3 reshape.149
  51.1 0.8 dynamic_slice.25
  51.9 1.8 fusion
  53.7 1.1 fusion.112
  54.7 1.3 constant_dynamic-slice_fusion
  56.1 0.0 copy-done.4
  56.1 2.2 multiply_convert_fusion
  58.3 38.9 %all-gather.7.cloned.1.call-done = bf16[4096,384]{1,0:T(8,128)(2,1)} async-done(((bf16[64,384]{1,0:T(8,128)(2,1)}), bf16[4096,384]{1,0:T(8,128)(2,1)}) %all-gather.7.cloned.1.call-update) | async-done | bytes 3145744 | tf_op jit(solution)/shard_map/all_gather | solution.py:56
  97.2 1.6 fusion.35
  98.8 1.6 fusion.36
  100.4 1.6 fusion.38
  102.1 1.6 fusion.37
  103.7 0.1 maximum_multiply_fusion
  103.8 4.5 %fusion.109 = (f32[3,128]{1,0:T(4,128)S(1)}, f32[3,128]{1,0:T(4,128)S(1)}, f32[3,128,256]{1,2,0:T(8,128)S(1)}) fusion(f32[3,128,256]{1,2,0:T(8,128)S(1)} %maximum_multiply_fusion, f32[256]{0:T(256)S(1)} %bitcast.119, f32[256]{0:T(256)S(1)} %bitcast.121, f32[256]{0:T(256)S(1)} %bitcast.122, f32[256]{0:T(256)S(1)} %bitcast.123, f32[256]{0:T(256)S(1)} %bitcast.124, ...), kind=kLoop, calls=%fused_computation.159 | loop fusion | flops 6290688 | bytes 821248 | tf_op jit(solution)/shard_map/reduce_sum | solution.py:135
  108.4 0.6 broadcast_in_dim.4
  109.0 8.6 %all-to-all-start = ((f32[8,1,768]{2,1,0:T(1,128)}), f32[8,1,768]{2,1,0:T(1,128)S(1)}, u32[]{:S(2)}, u32[]{:S(2)}) async-start(f32[8,1,768]{2,1,0:T(1,128)} %broadcast_in_dim.4), calls=%async_computation | async-start | bytes 49152 | tf_op jit(solution)/shard_map/all_to_all | solution.py:67
  117.6 1.3 fusion.111
  118.8 0.2 copy.58
  119.0 3.3 %all-to-all-done = f32[8,1,768]{2,1,0:T(1,128)S(1)} async-done(((f32[8,1,768]{2,1,0:T(1,128)}), f32[8,1,768]{2,1,0:T(1,128)S(1)}, u32[]{:S(2)}, u32[]{:S(2)}) %all-to-all-start) | async-done | bytes 24608 | tf_op jit(solution)/shard_map/all_to_all | solution.py:67
  122.3 0.2 multiply_convert_fusion.1
  122.5 0.6 convolution_convert_fusion
  123.2 0.1 copy.75
  123.3 0.0 copy-start.3
  123.3 23.8 %all_to_all.21 = bf16[8,384,256]{2,1,0:T(8,128)(2,1)S(1)} all-to-all(bf16[8,384,256]{2,1,0:T(8,128)(2,1)S(1)} %bitcast.98), channel_id=1, replica_groups=mesh['rep'=2,'fs'=32,'tp_0'=4,'tp_1'=2] {'tp_0','tp_1'}, dimensions={0} | all-to-all | bytes 3145728 | tf_op jit(solution)/shard_map/all_to_all | solution.py:90
  147.1 0.2 convert_reduce_fusion.1
  147.3 0.0 copy-done.3
  147.3 0.1 add_convert_fusion.2
  147.4 0.2 copy.61
  147.5 0.1 broadcast_in_dim.5
  147.7 0.0 copy-start.5
  147.7 24.1 %all_to_all.22 = bf16[8,384,256]{1,2,0:T(8,128)(2,1)S(1)} all-to-all(bf16[8,384,256]{1,2,0:T(8,128)(2,1)S(1)} %broadcast_in_dim.5), channel_id=1, replica_groups=mesh['rep'=2,'fs'=32,'tp_0'=4,'tp_1'=2] {'tp_0','tp_1'}, dimensions={0} | all-to-all | bytes 3145728 | tf_op jit(solution)/shard_map/all_to_all | solution.py:67
  171.8 0.4 multiply_reduce_fusion
  172.2 0.0 copy-done.5
  172.2 0.4 fusion.2
  172.6 17.4 %all-gather.9.cloned.1.call-done = bf16[4096,768]{1,0:T(8,128)(2,1)} async-done(((bf16[64,768]{1,0:T(8,128)(2,1)}), bf16[4096,768]{1,0:T(8,128)(2,1)}) %all-gather.9.cloned.1.call-update) | async-done | bytes 6291472 | tf_op jit(solution)/shard_map/all_gather | solution.py:56
  190.0 5.4 %fusion.6 = f32[384,2048]{1,0:T(8,128)} fusion(bf16[4096,768]{1,0:T(8,128)(2,1)} %all-gather.9.cloned.1.call-done, bf16[384,2048]{0,1:T(8,128)(2,1)S(1)} %fusion.2), kind=kOutput, calls=%fused_computation.47 | convolution fusion | flops 1208401920 | bytes 7864320 | tf_op jit(solution)/shard_map/dot_general | solution.py:106
  195.4 4.7 %add_convert_fusion = bf16[384,2048]{1,0:T(8,128)(2,1)S(1)} fusion(f32[384,2048]{1,0:T(8,128)} %fusion.6, bf16[4096,768]{1,0:T(8,128)(2,1)} %all-gather.9.cloned.1.call-done, bf16[384,2048]{0,1:T(8,128)(2,1)S(1)} %fusion.2), kind=kOutput, calls=%fused_computation.37 | convolution fusion | flops 1209974784 | bytes 9437184 | tf_op jit(solution)/shard_map/dot_general | solution.py:106
  200.2 0.1 copy.74
  200.3 26.5 %all_to_all.23 = bf16[8,384,256]{2,1,0:T(8,128)(2,1)S(1)} all-to-all(bf16[8,384,256]{2,1,0:T(8,128)(2,1)S(1)} %bitcast.99), channel_id=1, replica_groups=mesh['rep'=2,'fs'=32,'tp_0'=4,'tp_1'=2] {'tp_0','tp_1'}, dimensions={0} | all-to-all | bytes 3145728 | tf_op jit(solution)/shard_map/all_to_all | solution.py:90
  226.8 0.2 convert_reduce_fusion
  227.0 0.7 add_convert_fusion.1
  (6 shorter events, 0.1 us)
Async XLA Ops:
  6.5 0.8 copy-start
  6.5 90.6 %all-gather.7.cloned.1.call-start = ((), (), s32[]{:S(2)}) async-start(), calls=%async_computation.4 | async-start | bytes 3194880 | tf_op jit(solution)/shard_map/all_gather | solution.py:56
  8.7 181.3 %all-gather.9.cloned.1.call-start = ((), (), s32[]{:S(2)}) async-start(), calls=%async_computation.5 | async-start | bytes 6389760 | tf_op jit(solution)/shard_map/all_gather | solution.py:56
  32.6 13.2 %copy-start.1 = (bf16[4,2,192,256]{3,2,1,0:T(8,128)(2,1)}, bf16[4,2,192,256]{3,2,1,0:T(8,128)(2,1)S(1)}, u32[]{:S(2)}) copy-start(bf16[4,2,192,256]{3,2,1,0:T(8,128)(2,1)S(1)} %copy.52) | copy-start | bytes 2359300
  45.8 0.9 copy-start.2
  48.9 7.2 %copy-start.4 = (f32[2048]{0:T(1024)S(1)}, f32[2048]{0:T(1024)}, u32[]{:S(2)}) copy-start(f32[2048]{0:T(1024)} %param.11) | copy-start | bytes 24580
  109.0 13.3 %all-to-all-start = ((f32[8,1,768]{2,1,0:T(1,128)}), f32[8,1,768]{2,1,0:T(1,128)S(1)}, u32[]{:S(2)}, u32[]{:S(2)}) async-start(f32[8,1,768]{2,1,0:T(1,128)} %broadcast_in_dim.4), calls=%async_computation | async-start | bytes 49152 | tf_op jit(solution)/shard_map/all_to_all | solution.py:67
  123.3 24.0 %copy-start.3 = (bf16[384,256]{1,0:T(8,128)(2,1)S(1)}, bf16[384,256]{1,0:T(8,128)(2,1)}, u32[]{:S(2)}) copy-start(bf16[384,256]{1,0:T(8,128)(2,1)} %param.10) | copy-start | bytes 589828
  147.7 24.5 %copy-start.5 = (f32[2048]{0:T(1024)S(1)}, f32[2048]{0:T(1024)}, u32[]{:S(2)}) copy-start(f32[2048]{0:T(1024)} %param.17) | copy-start | bytes 24580
Sparse Core Ops, SparseCore 0:
  10.3 86.7 all-gather.6
  100.2 89.7 all-gather.8
where the time goes:
time: 236 us; the launch traced here: 235 us
  blocking collectives  109 us (46%)
  waiting for transfers between devices  59.6 us (25%)
  matrix products  17.2 us (7%)
  local copies, waits for them, and re-layouts  14.1 us (6%)
  between operations  13.6 us (6%)
  other arithmetic  12.5 us (5%)
  starting transfers between devices  8.62 us (4%)
    all_gather x2, waiting for transfers between devices, whole_halves(): pieces = lax.all_gather(mine, ('rep', 'fs'), axis=0, tiled=True)  56.3 us
    all_to_all x2, blocking collectives, summed_on_arrival(): lax.all_to_all(in_blocks(shard, dim, count), axis, 0, 0, tiled=True)  50.3 us
    all_gather x4, blocking collectives, gather_in_order(): pieces = lax.all_gather(pieces, axes[k])  34.5 us
    all_to_all x1, blocking collectives, copy_for_each(): return lax.all_to_all(copies, axis, split_axis=0, concat_axis=0, tiled=True)  24.1 us
    dot_general x3, matrix products, times_transposed(): lax.dot_general(left, right, (((1,), (1,)), ((), ())), preferred_element_...  10.8 us
    all_to_all x1, starting transfers between devices, copy_for_each(): return lax.all_to_all(copies, axis, split_axis=0, concat_axis=0, tiled=True)  8.58 us
  transfers between devices with their start and end apart: 3, of which 3 were waited for; matrix products, arithmetic and copies ran while one was open for 13% of the time, Pallas kernels for 0%

commit v1 on v0

--- a/solution.py
+++ b/solution.py
@@ -53,7 +53,10 @@
 
 def whole_halves(weights):
     mine = jnp.concatenate([half_of(w) for w in weights], axis=1)
-    pieces = lax.all_gather(mine, ("rep", "fs"), axis=0, tiled=True)
+    pieces = jnp.concatenate(
+        lax.all_to_all(jnp.stack([mine] * lax.axis_size(("rep", "fs"))), ("rep", "fs"), 0, 0),
+        axis=0,
+    )
     pieces = pieces.reshape(2, -1, mine.shape[1])
     ends, at = ([], 0)
     for w in weights[:-1]:

time: 236 us -> 454 us (1.92)
  the two profiles are of different devices: /device:TPU:1 before, /device:TPU:40 now
where the time goes in v1:
time: 454 us; the launch traced here: 453 us
  waiting for transfers between devices  286 us (63%)
  blocking collectives  78.9 us (17%)
  starting transfers between devices  32.2 us (7%)
  local copies, waits for them, and re-layouts  28.7 us (6%)
  matrix products  14.2 us (3%)
  other arithmetic  12.4 us (3%)
    all_to_all x2, waiting for transfers between devices, whole_halves(): lax.all_to_all(jnp.stack([mine] * lax.axis_size(('rep', 'fs'))), ('rep',...  261 us
    all_to_all x2, blocking collectives, summed_on_arrival(): lax.all_to_all(in_blocks(shard, dim, count), axis, 0, 0, tiled=True)  48 us
    all_gather x4, blocking collectives, gather_in_order(): pieces = lax.all_gather(pieces, axes[k])  30.8 us
    all_to_all x2, waiting for transfers between devices, copy_for_each(): return lax.all_to_all(copies, axis, split_axis=0, concat_axis=0, tiled=True)  24.8 us
    all_to_all x2, starting transfers between devices, whole_halves(): lax.all_to_all(jnp.stack([mine] * lax.axis_size(('rep', 'fs'))), ('rep',...  24.2 us
    dot_general x3, matrix products, times_transposed(): lax.dot_general(left, right, (((1,), (1,)), ((), ())), preferred_element_...  11.9 us
  transfers between devices with their start and end apart: 4, of which 4 were waited for; matrix products, arithmetic and copies ran while one was open for 3% of the time, Pallas kernels for 0%

profile of v1, /device:TPU:40, one launch (start us, length us, event | category | flops | bytes accessed | tf_op | source)
XLA Modules:
  0.0 452.7 jit_solution(2299130367446912522)
XLA Ops:
  0.0 0.0 copy-start
  0.0 0.8 copy-done
  0.8 0.7 constant_dynamic-slice_fusion.3
  1.5 2.2 stack.4
  3.7 16.4 %all-to-all-start = ((bf16[64,64,384]{2,1,0:T(8,128)(2,1)}), bf16[64,64,384]{2,1,0:T(8,128)(2,1)}, u32[]{:S(2)}, u32[]{:S(2)}) async-start(bf16[64,64,384]{2,1,0:T(8,128)(2,1)} %stack.4), calls=%async_computation | async-start | bytes 6291456 | tf_op jit(solution)/shard_map/all_to_all | solution.py:57
  20.1 0.0 copy-done.4
  20.2 12.9 %all-gather = bf16[768,256]{1,0:T(8,128)(2,1)S(1)} all-gather(bf16[192,256]{1,0:T(8,128)(2,1)S(1)} %get-tuple-element.43), channel_id=2, replica_groups=mesh['rep'=2,'fs'=32,'tp_0'=4,'tp_1'=2] {'tp_0'}, dimensions={0}, use_global_device_ids=true | all-gather | bytes 491520 | tf_op jit(solution)/shard_map/all_gather | solution.py:24
  33.0 2.4 all-gather.1
  35.4 0.1 copy.51
  35.5 0.0 copy-start.1
  35.5 1.9 all-gather.2
  37.4 13.7 %all-gather.3 = bf16[8,192,256]{2,1,0:T(8,128)(2,1)S(1)} all-gather(bf16[2,192,256]{2,1,0:T(8,128)(2,1)S(1)} %bitcast.116), channel_id=5, replica_groups=mesh['rep'=2,'fs'=32,'tp_0'=4,'tp_1'=2] {'tp_0'}, dimensions={0}, use_global_device_ids=true | all-gather | bytes 983040 | tf_op jit(solution)/shard_map/all_gather | solution.py:24
  51.1 0.0 copy-done.1
  51.1 0.9 copy-done.2
  52.0 0.3 convert_bitcast_fusion
  52.2 1.8 copy.52
  54.1 2.4 reshape.151
  56.5 1.8 fusion
  58.2 1.1 fusion.113
  59.3 1.3 constant_dynamic-slice_fusion
  60.7 0.0 copy-done.8
  60.7 2.2 multiply_convert_fusion
  62.9 52.8 %all-to-all-done = bf16[64,64,384]{2,1,0:T(8,128)(2,1)} async-done(((bf16[64,64,384]{2,1,0:T(8,128)(2,1)}), bf16[64,64,384]{2,1,0:T(8,128)(2,1)}, u32[]{:S(2)}, u32[]{:S(2)}) %all-to-all-start) | async-done | bytes 3145760 | tf_op jit(solution)/shard_map/all_to_all | solution.py:57
  115.7 2.2 fusion.112
  117.9 0.0 copy-start.3
  118.0 0.6 fusion.37
  118.6 0.6 fusion.35
  119.2 0.0 copy-done.3
  119.2 0.6 fusion.38
  119.8 0.6 fusion.36
  120.3 0.1 maximum_multiply_fusion
  120.5 4.5 %fusion.109 = (f32[3,128]{1,0:T(4,128)S(1)}, f32[3,128]{1,0:T(4,128)S(1)}, f32[3,128,256]{1,2,0:T(8,128)S(1)}) fusion(f32[3,128,256]{1,2,0:T(8,128)S(1)} %maximum_multiply_fusion, f32[256]{0:T(256)S(1)} %bitcast.131, f32[256]{0:T(256)S(1)} %bitcast.133, f32[256]{0:T(256)S(1)} %bitcast.134, f32[256]{0:T(256)S(1)} %bitcast.135, f32[256]{0:T(256)S(1)} %bitcast.136, ...), kind=kLoop, calls=%fused_computation.159 | loop fusion | flops 6290688 | bytes 821248 | tf_op jit(solution)/shard_map/reduce_sum | solution.py:138
  125.0 0.6 broadcast_in_dim.4
  125.7 4.3 all-to-all-start.1
  130.0 0.8 dynamic_slice.25
  130.7 1.1 split.53
  131.8 0.2 copy.57
  132.0 3.4 all-to-all-done.1
  135.4 0.2 multiply_convert_fusion.1
  135.6 0.6 convolution_convert_fusion
  136.2 0.1 copy.74
  136.3 24.0 %all_to_all.31 = bf16[8,384,256]{2,1,0:T(8,128)(2,1)S(1)} all-to-all(bf16[8,384,256]{2,1,0:T(8,128)(2,1)S(1)} %bitcast.102), channel_id=1, replica_groups=mesh['rep'=2,'fs'=32,'tp_0'=4,'tp_1'=2] {'tp_0','tp_1'}, dimensions={0} | all-to-all | bytes 3145728 | tf_op jit(solution)/shard_map/all_to_all | solution.py:93
  160.4 0.2 convert_reduce_fusion.1
  160.6 0.7 copy-done.5
  161.3 0.2 copy.60
  161.5 1.3 broadcast_in_dim.5
  162.8 3.7 all-to-all-start.3
  166.5 0.0 copy-done.6
  166.5 0.0 copy-done.7
  166.6 21.4 %all-to-all-done.3 = bf16[8,384,256]{1,2,0:T(8,128)(2,1)S(1)} async-done(((bf16[8,384,256]{1,2,0:T(8,128)(2,1)}), bf16[8,384,256]{1,2,0:T(8,128)(2,1)S(1)}, u32[]{:S(2)}, u32[]{:S(2)}) %all-to-all-start.3) | async-done | bytes 1572896 | tf_op jit(solution)/shard_map/all_to_all | solution.py:70
  188.0 3.4 stack.5
  191.4 7.8 %all-to-all-start.4 = ((bf16[64,64,768]{2,1,0:T(8,128)(2,1)}), bf16[64,64,768]{2,1,0:T(8,128)(2,1)}, u32[]{:S(2)}, u32[]{:S(2)}) async-start(bf16[64,64,768]{2,1,0:T(8,128)(2,1)} %stack.5), calls=%async_computation.4 | async-start | bytes 12582912 | tf_op jit(solution)/shard_map/all_to_all | solution.py:57
  199.2 0.0 copy-start.9
  199.2 0.4 multiply_reduce_fusion
  199.6 0.3 copy-done.9
  199.9 1.6 fusion.2
  201.5 208.3 %all-to-all-done.4 = bf16[64,64,768]{2,1,0:T(8,128)(2,1)} async-done(((bf16[64,64,768]{2,1,0:T(8,128)(2,1)}), bf16[64,64,768]{2,1,0:T(8,128)(2,1)}, u32[]{:S(2)}, u32[]{:S(2)}) %all-to-all-start.4) | async-done | bytes 6291488 | tf_op jit(solution)/shard_map/all_to_all | solution.py:57
  409.8 5.1 %fusion.111 = (bf16[32,64,768]{2,1,0:T(8,128)(2,1)S(1)}, bf16[32,64,768]{2,1,0:T(8,128)(2,1)}) fusion(bf16[64,64,768]{2,1,0:T(8,128)(2,1)} %all-to-all-done.4), kind=kLoop, calls=%fused_computation.160 | loop fusion | bytes 12582912 | tf_op jit(solution)/shard_map/slice | solution.py:65
  414.9 5.9 %fusion.6 = f32[384,2048]{1,0:T(8,128)} fusion(bf16[2048,768]{1,0:T(8,128)(2,1)} %bitcast.113, bf16[384,2048]{0,1:T(8,128)(2,1)} %fusion.2), kind=kOutput, calls=%fused_computation.47 | convolution fusion | flops 1208401920 | bytes 7864320 | tf_op jit(solution)/shard_map/dot_general | solution.py:109
  420.8 5.4 %add_convert_fusion = bf16[384,2048]{1,0:T(8,128)(2,1)} fusion(f32[384,2048]{1,0:T(8,128)} %fusion.6, bf16[2048,768]{1,0:T(8,128)(2,1)S(1)} %bitcast.112, bf16[384,2048]{0,1:T(8,128)(2,1)} %fusion.2), kind=kOutput, calls=%fused_computation.37 | convolution fusion | flops 1209974784 | bytes 9437184 | tf_op jit(solution)/shard_map/dot_general | solution.py:109
  426.2 1.5 copy.73
  427.7 24.0 %all_to_all.32 = bf16[8,384,256]{2,1,0:T(8,128)(2,1)S(1)} all-to-all(bf16[8,384,256]{2,1,0:T(8,128)(2,1)S(1)} %bitcast.103), channel_id=1, replica_groups=mesh['rep'=2,'fs'=32,'tp_0'=4,'tp_1'=2] {'tp_0','tp_1'}, dimensions={0} | all-to-all | bytes 3145728 | tf_op jit(solution)/shard_map/all_to_all | solution.py:93
  451.7 0.2 convert_reduce_fusion
  452.0 0.7 add_convert_fusion.1
  (18 shorter events, 0.2 us)
Async XLA Ops:
  0.0 0.8 copy-start
  3.7 16.4 %copy-start.4 = (bf16[384,256]{1,0:T(8,128)(2,1)S(1)}, bf16[384,256]{1,0:T(8,128)(2,1)}, u32[]{:S(2)}) copy-start(bf16[384,256]{1,0:T(8,128)(2,1)} %param.10) | copy-start | bytes 589828
  3.7 112.0 %all-to-all-start = ((bf16[64,64,384]{2,1,0:T(8,128)(2,1)}), bf16[64,64,384]{2,1,0:T(8,128)(2,1)}, u32[]{:S(2)}, u32[]{:S(2)}) async-start(bf16[64,64,384]{2,1,0:T(8,128)(2,1)} %stack.4), calls=%async_computation | async-start | bytes 6291456 | tf_op jit(solution)/shard_map/all_to_all | solution.py:57
  35.5 15.6 %copy-start.1 = (bf16[4,2,192,256]{3,2,1,0:T(8,128)(2,1)}, bf16[4,2,192,256]{3,2,1,0:T(8,128)(2,1)S(1)}, u32[]{:S(2)}) copy-start(bf16[4,2,192,256]{3,2,1,0:T(8,128)(2,1)S(1)} %copy.51) | copy-start | bytes 2359300
  51.1 0.9 copy-start.2
  56.5 4.2 copy-start.8
  117.9 1.2 copy-start.3
  125.7 9.7 %all-to-all-start.1 = ((f32[8,1,768]{2,1,0:T(1,128)}), f32[8,1,768]{2,1,0:T(1,128)S(1)}, u32[]{:S(2)}, u32[]{:S(2)}) async-start(f32[8,1,768]{2,1,0:T(1,128)} %broadcast_in_dim.4), calls=%async_computation.1 | async-start | bytes 49152 | tf_op jit(solution)/shard_map/all_to_all | solution.py:70
  160.4 0.9 copy-start.5
  162.8 3.7 copy-start.6
  162.8 3.7 copy-start.7
  162.8 25.2 %all-to-all-start.3 = ((bf16[8,384,256]{1,2,0:T(8,128)(2,1)}), bf16[8,384,256]{1,2,0:T(8,128)(2,1)S(1)}, u32[]{:S(2)}, u32[]{:S(2)}) async-start(bf16[8,384,256]{1,2,0:T(8,128)(2,1)} %broadcast_in_dim.5), calls=%async_computation.3 | async-start | bytes 3145728 | tf_op jit(solution)/shard_map/all_to_all | solution.py:70
  191.4 218.4 %all-to-all-start.4 = ((bf16[64,64,768]{2,1,0:T(8,128)(2,1)}), bf16[64,64,768]{2,1,0:T(8,128)(2,1)}, u32[]{:S(2)}, u32[]{:S(2)}) async-start(bf16[64,64,768]{2,1,0:T(8,128)(2,1)} %stack.5), calls=%async_computation.4 | async-start | bytes 12582912 | tf_op jit(solution)/shard_map/all_to_all | solution.py:57
  199.2 0.7 copy-start.9
